TPU v7x, 32 devices: a whole 2x2x4 slice. The times are simulated.
32 devices in a mesh: grp: 2 (over y), ra: 4 (over z), cb: 2 (over x), dp: 2 (over core).
Axes of the slice: x: 2, y: 2, z: 4, core: 2. Of those that a mesh axis runs over, the one named last changes fastest.
Arguments:
- tokens: bfloat16 [256, 2048], P(('grp', 'dp'), 'ra'), parts along dimension 0, may hold values from -51 to 51
- first_gain: float32 [2048], P('ra'), may hold values from 0.1 to 1.9
- first_gate: float32 [2048, 5632], P('ra', 'cb'), may hold values from -0.125 to 0.125
- first_up: float32 [2048, 5632], P('ra', 'cb'), may hold values from -0.125 to 0.125
- first_down: float32 [5632, 2048], P('cb', 'ra'), may hold values from -0.078125 to 0.078125
- first_gate_scale: float32 [5632], P('cb'), may hold values from 0.1 to 1.9
- first_up_scale: float32 [5632], P('cb'), may hold values from 0.1 to 1.9
- first_down_scale: float32 [2048], P('ra'), may hold values from 0.1 to 1.9
- second_gain: float32 [2048], P('ra'), may hold values from 0.1 to 1.9
- second_gate: float32 [2048, 5632], P('ra', 'cb'), may hold values from -0.125 to 0.125
- second_up: float32 [2048, 5632], P('ra', 'cb'), may hold values from -0.125 to 0.125
- second_down: float32 [5632, 2048], P('cb', 'ra'), may hold values from -0.078125 to 0.078125
- second_gate_scale: float32 [5632], P('cb'), may hold values from 0.1 to 1.9
- second_up_scale: float32 [5632], P('cb'), may hold values from 0.1 to 1.9
- second_down_scale: float32 [2048], P('ra'), may hold values from 0.1 to 1.9
Outputs:
- result: bfloat16 [256, 2048], P(('grp', 'dp'), 'ra'), parts along dimension 0
There are 2 independent parts, one for each index of `grp`. A program takes and returns all parts, laid end to end along the dimension named above; an argument that names none is the same for every part. Nothing has to cross between parts.
All inputs are finite; a program needn't handle non-finite values.
Results may differ from a plain program's by a relative error of at most 0.04.
Values may be sent and summed in bfloat16 or wider, within the bound.
A program may use at most 64 MiB of HBM per device.

v0:
```python
import jax
import jax.numpy as jnp
from jax import lax
from jax.sharding import PartitionSpec as P

D = 2048


EPS = 1e-06


def sublayer(values, gain, w_gate, w_up, w_down, gate_scale, up_scale, down_scale):
    floats = values.astype(jnp.float32)
    squares_row = jnp.sum(floats * floats, axis=1)
    scaled = (floats * gain).astype(jnp.bfloat16)
    gate_part = jnp.dot(scaled, w_gate.astype(jnp.bfloat16), preferred_element_type=jnp.float32)
    up_part = jnp.dot(scaled, w_up.astype(jnp.bfloat16), preferred_element_type=jnp.float32)
    total = lax.psum(squares_row, "ra")
    inverse = lax.rsqrt(total / D + EPS)[:, None]
    gate_sum, up_sum = (
        lax.psum(gate_part.astype(jnp.bfloat16), "ra").astype(jnp.float32),
        lax.psum(up_part.astype(jnp.bfloat16), "ra").astype(jnp.float32),
    )
    hidden = (jax.nn.silu(gate_sum * gate_scale * inverse) * (up_sum * up_scale * inverse)).astype(
        jnp.bfloat16
    )
    down_part = jnp.dot(hidden, w_down.astype(jnp.bfloat16), preferred_element_type=jnp.float32)
    down = lax.psum(down_part.astype(jnp.bfloat16), "cb").astype(jnp.float32)
    return (0.3 * floats + 0.5 * down * down_scale).astype(jnp.bfloat16)


def per_device(
    tokens,
    first_gain,
    first_gate,
    first_up,
    first_down,
    first_gate_scale,
    first_up_scale,
    first_down_scale,
    second_gain,
    second_gate,
    second_up,
    second_down,
    second_gate_scale,
    second_up_scale,
    second_down_scale,
):
    middle = sublayer(
        tokens,
        first_gain,
        first_gate,
        first_up,
        first_down,
        first_gate_scale,
        first_up_scale,
        first_down_scale,
    )
    return sublayer(
        middle,
        second_gain,
        second_gate,
        second_up,
        second_down,
        second_gate_scale,
        second_up_scale,
        second_down_scale,
    )


def solution(mesh):
    in_specs = (
        P(("grp", "dp"), "ra"),
        P("ra"),
        P("ra", "cb"),
        P("ra", "cb"),
        P("cb", "ra"),
        P("cb"),
        P("cb"),
        P("ra"),
        P("ra"),
        P("ra", "cb"),
        P("ra", "cb"),
        P("cb", "ra"),
        P("cb"),
        P("cb"),
        P("ra"),
    )
    out_specs = P(("grp", "dp"), "ra")
    return jax.shard_map(
        per_device, mesh=mesh, in_specs=in_specs, out_specs=out_specs, check_vma=False
    )
```

profile of v0, /device:TPU:0, one launch (start us, length us, event | category | flops | bytes accessed | tf_op | source)
XLA Modules:
  0.0 166.8 jit_solution(15138607486310088870)
XLA Ops:
  6.5 0.0 copy-start.1
  6.5 0.0 copy-start.6
  6.5 0.0 copy-start.3
  6.5 0.0 copy-start.2
  6.5 0.0 all-reduce.13.cloned.1.call-start
  6.6 0.0 copy-start
  6.6 4.2 %convolution_convert_fusion.2 = bf16[64,2816]{1,0:T(8,128)(2,1)} fusion(f32[512,2816]{1,0:T(8,128)} %param.18, bf16[64,512]{1,0:T(8,128)(2,1)} %param.15, f32[512]{0:T(512)} %param.16), kind=kOutput, calls=%fused_computation.2 | convolution fusion | flops 186269696 | bytes 6195200 | tf_op jit(solution)/shard_map/dot_general | solution.py:17
  10.8 0.0 copy-done.1
  10.8 0.0 copy-done.6
  10.8 0.2 copy-done
  11.0 0.0 copy-start.8
  11.0 0.0 copy-start.7
  11.0 1.4 convolution_convert_fusion.3
  12.4 0.0 all-reduce.13.cloned.1.call-update
  12.4 0.0 all-reduce.7.cloned.1.call-start
  12.4 0.1 fusion.25
  12.5 13.6 %psum.57 = f32[64]{0:T(128)S(1)} all-reduce(f32[64]{0:T(128)S(1)} %fusion.25), channel_id=1, replica_groups=mesh['grp'=2,'ra'=4,'cb'=2,'dp'=2] {'ra'}, use_global_device_ids=true, to_apply=%region_2.0 | all-reduce | flops 64 | bytes 512 | tf_op jit(solution)/shard_map/psum | solution.py:18
  26.1 31.2 %all-reduce.13.cloned.1.call-done = (bf16[64,2816]{1,0:T(8,128)(2,1)}, bf16[64,2816]{1,0:T(8,128)(2,1)}) async-done(((bf16[64,2816]{1,0:T(8,128)(2,1)}, bf16[64,2816]{1,0:T(8,128)(2,1)}), (bf16[64,2816]{1,0:T(8,128)(2,1)}, bf16[64,2816]{1,0:T(8,128)(2,1)})) %all-reduce.13.cloned.1.call-update) | async-done | bytes 720912 | tf_op jit(solution)/shard_map/psum | solution.py:22
  57.3 0.0 copy-done.3
  57.3 0.0 copy-done.2
  57.3 4.3 %fusion.8 = bf16[64,512]{1,0:T(8,128)(2,1)} fusion(f32[2816,512]{1,0:T(8,128)} %param.19, bf16[64,2816]{1,0:T(8,128)(2,1)} %get-tuple-element.7, bf16[64,2816]{1,0:T(8,128)(2,1)} %get-tuple-element.8, f32[2816]{0:T(1024)S(1)} %copy-done.2, f32[64]{0:T(128)S(1)} %add_rsqrt_fusion.1, f32[2816]{0:T(1024)S(1)} %copy-done.3), kind=kOutput, calls=%fused_computation.12 | convolution fusion | flops 188186624 | bytes 6576384 | tf_op jit(solution)/shard_map/dot_general | solution.py:27
  61.7 0.0 all-reduce.7.cloned.1.call-update
  61.7 0.0 all-reduce.11.cloned.1.call-start
  61.7 0.0 copy-done.8
  61.8 20.6 %all-reduce.7.cloned.1.call-done = bf16[64,512]{1,0:T(8,128)(2,1)} async-done(((bf16[64,512]{1,0:T(8,128)(2,1)}), bf16[64,512]{1,0:T(8,128)(2,1)}) %all-reduce.7.cloned.1.call-update) | async-done | bytes 65552 | tf_op jit(solution)/shard_map/psum | solution.py:28
  82.3 1.0 fusion.29
  83.3 0.0 copy-done.7
  83.3 0.0 copy-start.4
  83.3 0.0 copy-start.5
  83.3 4.0 %convolution_convert_fusion = bf16[64,2816]{1,0:T(8,128)(2,1)} fusion(f32[512,2816]{1,0:T(8,128)} %param.25, bf16[64,512]{1,0:T(8,128)(2,1)S(1)} %get-tuple-element.10, f32[512]{0:T(512)S(1)} %copy-done.7), kind=kOutput, calls=%fused_computation | convolution fusion | flops 186269696 | bytes 6195200 | tf_op jit(solution)/shard_map/dot_general | solution.py:17
  87.3 0.0 copy-start.9
  87.3 4.0 %convolution_convert_fusion.1 = bf16[64,2816]{1,0:T(8,128)(2,1)} fusion(f32[512,2816]{1,0:T(8,128)} %param.24, bf16[64,512]{1,0:T(8,128)(2,1)S(1)} %get-tuple-element.10, f32[512]{0:T(512)S(1)} %copy-done.7), kind=kOutput, calls=%fused_computation.1 | convolution fusion | flops 186269696 | bytes 6195200 | tf_op jit(solution)/shard_map/dot_general | solution.py:16
  91.4 0.0 all-reduce.11.cloned.1.call-update
  91.4 0.0 all-reduce.9.cloned.1.call-start
  91.4 12.0 %psum.61 = f32[64]{0:T(128)S(1)} all-reduce(f32[64]{0:T(128)S(1)} %get-tuple-element.9), channel_id=1, replica_groups=mesh['grp'=2,'ra'=4,'cb'=2,'dp'=2] {'ra'}, use_global_device_ids=true, to_apply=%region_7.8 | all-reduce | flops 64 | bytes 512 | tf_op jit(solution)/shard_map/psum | solution.py:18
  103.5 30.3 %all-reduce.11.cloned.1.call-done = (bf16[64,2816]{1,0:T(8,128)(2,1)}, bf16[64,2816]{1,0:T(8,128)(2,1)}) async-done(((bf16[64,2816]{1,0:T(8,128)(2,1)}, bf16[64,2816]{1,0:T(8,128)(2,1)}), (bf16[64,2816]{1,0:T(8,128)(2,1)}, bf16[64,2816]{1,0:T(8,128)(2,1)})) %all-reduce.11.cloned.1.call-update) | async-done | bytes 720912 | tf_op jit(solution)/shard_map/psum | solution.py:22
  133.8 0.0 copy-done.4
  133.8 0.0 copy-done.5
  133.8 4.3 %fusion.11 = bf16[64,512]{1,0:T(8,128)(2,1)} fusion(f32[2816,512]{1,0:T(8,128)} %param.26, bf16[64,2816]{1,0:T(8,128)(2,1)} %get-tuple-element.5, bf16[64,2816]{1,0:T(8,128)(2,1)} %get-tuple-element.6, f32[2816]{0:T(1024)S(1)} %copy-done.4, f32[64]{0:T(128)S(1)} %add_rsqrt_fusion, f32[2816]{0:T(1024)S(1)} %copy-done.5), kind=kOutput, calls=%fused_computation.13 | convolution fusion | flops 188186624 | bytes 6576384 | tf_op jit(solution)/shard_map/dot_general | solution.py:27
  138.1 0.0 all-reduce.9.cloned.1.call-update
  138.1 0.0 copy-done.9
  138.2 20.6 %all-reduce.9.cloned.1.call-done = bf16[64,512]{1,0:T(8,128)(2,1)} async-done(((bf16[64,512]{1,0:T(8,128)(2,1)}), bf16[64,512]{1,0:T(8,128)(2,1)}) %all-reduce.9.cloned.1.call-update) | async-done | bytes 65552 | tf_op jit(solution)/shard_map/psum | solution.py:28
  158.8 1.5 fusion.27
  (4 shorter events, 0.0 us)
Async XLA Ops:
  6.5 4.3 %copy-start.1 = (bf16[64,512]{1,0:T(8,128)(2,1)S(1)}, bf16[64,512]{1,0:T(8,128)(2,1)}, u32[]{:S(2)}) copy-start(bf16[64,512]{1,0:T(8,128)(2,1)} %param.15) | copy-start | bytes 196612
  6.5 4.3 %copy-start.6 = (f32[512]{0:T(512)S(1)}, f32[512]{0:T(512)}, u32[]{:S(2)}) copy-start(f32[512]{0:T(512)} %param.16) | copy-start | bytes 6148
  6.5 50.8 %copy-start.3 = (f32[2816]{0:T(1024)S(1)}, f32[2816]{0:T(1024)}, u32[]{:S(2)}) copy-start(f32[2816]{0:T(1024)} %param.20) | copy-start | bytes 33796
  6.5 50.8 %copy-start.2 = (f32[2816]{0:T(1024)S(1)}, f32[2816]{0:T(1024)}, u32[]{:S(2)}) copy-start(f32[2816]{0:T(1024)} %param.21) | copy-start | bytes 33796
  6.5 50.8 %all-reduce.13.cloned.1.call-start = ((), (), s32[]{:S(2)}) async-start(), calls=%async_computation.3 | async-start | bytes 1441792 | tf_op jit(solution)/shard_map/psum | solution.py:22
  6.6 4.4 %copy-start = (f32[512,2816]{1,0:T(8,128)S(1)}, f32[512,2816]{1,0:T(8,128)}, u32[]{:S(2)}) copy-start(f32[512,2816]{1,0:T(8,128)} %param.17) | copy-start | bytes 17301508
  11.0 50.8 %copy-start.8 = (f32[512]{0:T(512)S(1)}, f32[512]{0:T(512)}, u32[]{:S(2)}) copy-start(f32[512]{0:T(512)} %param.22) | copy-start | bytes 6148
  11.0 72.3 %copy-start.7 = (f32[512]{0:T(512)S(1)}, f32[512]{0:T(512)}, u32[]{:S(2)}) copy-start(f32[512]{0:T(512)} %param.23) | copy-start | bytes 6148
  12.4 69.9 %all-reduce.7.cloned.1.call-start = ((), (), s32[]{:S(2)}) async-start(), calls=%async_computation | async-start | bytes 131072 | tf_op jit(solution)/shard_map/psum | solution.py:28
  61.7 72.1 %all-reduce.11.cloned.1.call-start = ((), (), s32[]{:S(2)}) async-start(), calls=%async_computation.2 | async-start | bytes 1441792 | tf_op jit(solution)/shard_map/psum | solution.py:22
  83.3 50.5 %copy-start.4 = (f32[2816]{0:T(1024)S(1)}, f32[2816]{0:T(1024)}, u32[]{:S(2)}) copy-start(f32[2816]{0:T(1024)} %param.28) | copy-start | bytes 33796
  83.3 50.4 %copy-start.5 = (f32[2816]{0:T(1024)S(1)}, f32[2816]{0:T(1024)}, u32[]{:S(2)}) copy-start(f32[2816]{0:T(1024)} %param.27) | copy-start | bytes 33796
  87.3 50.8 %copy-start.9 = (f32[512]{0:T(512)S(1)}, f32[512]{0:T(512)}, u32[]{:S(2)}) copy-start(f32[512]{0:T(512)} %param.29) | copy-start | bytes 6148
  91.4 67.4 %all-reduce.9.cloned.1.call-start = ((), (), s32[]{:S(2)}) async-start(), calls=%async_computation.1 | async-start | bytes 131072 | tf_op jit(solution)/shard_map/psum | solution.py:28
Sparse Core Ops, SparseCore 0:
  12.5 44.7 all-reduce.12
  61.8 20.4 all-reduce.6
  91.5 42.2 all-reduce.10
  138.3 20.4 all-reduce.8
where the time goes:
time: 167 us
  waiting for transfers between devices  103 us (62%)
  blocking collectives  25.6 us (15%)
  matrix products  22.3 us (13%)
  between operations  13.2 us (8%)
  other arithmetic  2.6 us (2%)
    psum x2, waiting for transfers between devices, sublayer(): lax.psum(up_part.astype(jnp.bfloat16), 'ra').astype(jnp.float32)  61.5 us
    psum x2, waiting for transfers between devices, sublayer(): down = lax.psum(down_part.astype(jnp.bfloat16), 'cb').astype(jnp.float32)  41.2 us
    psum x2, blocking collectives, sublayer(): total = lax.psum(squares_row, 'ra')  25.6 us
    dot_general x2, matrix products, sublayer(): jnp.dot(hidden, w_down.astype(jnp.bfloat16), preferred_element_type=jnp.f...  8.7 us
    dot_general x2, matrix products, sublayer(): jnp.dot(scaled, w_up.astype(jnp.bfloat16), preferred_element_type=jnp.flo...  8.2 us
    dot_general x2, matrix products, sublayer(): jnp.dot(scaled, w_gate.astype(jnp.bfloat16), preferred_element_type=jnp.f...  5.4 us
  transfers between devices with their start and end apart: 4, of which 4 were waited for; matrix products, arithmetic and copies ran while one was open for 0% of the time, Pallas kernels for 0%

commit v1 on v0

v1 whole, which is shorter than its diff:
```python
import functools

import jax
import jax.numpy as jnp
from jax import lax
from jax.experimental import pallas as pl
from jax.experimental.pallas import tpu as pltpu
from jax.sharding import PartitionSpec as P

EPS = 1e-06
MESH = pl.DeviceIdType.MESH
LANES = 128
LAG_SUM = 3
LAG_HID = 3


def kernel(dims, *refs):
    n, m, rows, width, units, total_width = dims
    (tokens, gain0, gate0, up0, down0, gs0, us0, ds0, gain1, gate1, up1, down1, gs1, us1, ds1) = refs[:15]
    out = refs[15]
    (values, scaled, gains, dscales, gscales, uscales, w_gu, w_down, own, sum_out, sum_in, hid, acc,
     down_in, squares, inverse, small_sem, gate_sem, up_sem, down_sem, sum_ss, sum_rs, hid_ss, hid_rs,
     part_ss, part_rs, sq_ss, sq_rs) = refs[16:]
    gate, up, down = (gate0, gate1), (up0, up1), (down0, down1)
    bf16, f32 = jnp.bfloat16, jnp.float32

    z, x = lax.axis_index("ra"), lax.axis_index("cb")
    blocks = units // LANES
    counts = (blocks - blocks // 2, blocks // 2)
    starts = (0, counts[0])
    place = (n - 1 - z, z)
    step = (-1, 1)
    pairs = counts[0]
    slots = max(2 * pairs, pairs + LAG_SUM * (n - 1) + LAG_HID * (n - 1))

    def copy_small():
        found = []
        for i, (src, dst) in enumerate((
            (tokens, values), (gain0, gains.at[0]), (gs0, gscales.at[0]), (us0, uscales.at[0]), (ds0, dscales.at[0]),
            (gain1, gains.at[1]), (gs1, gscales.at[1]), (us1, uscales.at[1]), (ds1, dscales.at[1]),
        )):
            found.append(pltpu.make_async_copy(src, dst, small_sem.at[i]))
        return found

    def columns(c):
        return pl.ds(pl.multiple_of(c * LANES, LANES), LANES)

    def gate_copy(l, c):
        return pltpu.make_async_copy(gate[l].at[:, columns(c)], w_gu.at[l, c, :, pl.ds(0, LANES)], gate_sem.at[l, c])

    def up_copy(l, c):
        return pltpu.make_async_copy(up[l].at[:, columns(c)], w_gu.at[l, c, :, pl.ds(LANES, LANES)], up_sem.at[l, c])

    def down_copy(l, c):
        return pltpu.make_async_copy(down[l].at[columns(c), :], w_down.at[l, c], down_sem.at[l, c])

    def sum_copy(l, c, d):
        return pltpu.make_async_remote_copy(
            src_ref=sum_out.at[l, c], dst_ref=sum_in.at[l, c], send_sem=sum_ss.at[l, c], recv_sem=sum_rs.at[l, c],
            device_id={"ra": z + step[d]}, device_id_type=MESH)

    def hid_copy(l, c, d):
        return pltpu.make_async_remote_copy(
            src_ref=hid.at[l, c], dst_ref=hid.at[l, c], send_sem=hid_ss.at[l, c], recv_sem=hid_rs.at[l, c],
            device_id={"ra": z - step[d]}, device_id_type=MESH)

    def part_copy(l, o, sender):
        return pltpu.make_async_remote_copy(
            src_ref=down_in.at[l, sender], dst_ref=down_in.at[l, sender], send_sem=part_ss.at[l, o],
            recv_sem=part_rs.at[l, sender], device_id={"cb": lax.rem(x + o, m)}, device_id_type=MESH)

    def sq_copy(l, end, sender):
        return pltpu.make_async_remote_copy(
            src_ref=squares.at[l, sender], dst_ref=squares.at[l, sender], send_sem=sq_ss.at[l, end],
            recv_sem=sq_rs.at[l, sender], device_id={"ra": end * (n - 1)}, device_id_type=MESH)

    def each_pair(i, act):
        for d in range(2):
            if counts[0] == counts[1]:
                act(starts[d] + i)
            else:
                @pl.when(i < counts[d])
                def _():
                    act(starts[d] + i)

    small = copy_small()
    for copy in small:
        copy.start()

    def start_first(i, carry):
        def act(c):
            gate_copy(0, c).start()
            up_copy(0, c).start()
        each_pair(i, act)
        return carry

    lax.fori_loop(0, pairs, start_first, 0)

    barrier = pltpu.get_barrier_semaphore()
    for o in range(1, n):
        pl.semaphore_signal(barrier, inc=1, device_id={"ra": lax.rem(z + o, n)}, device_id_type=MESH)
    for o in range(1, m):
        pl.semaphore_signal(barrier, inc=1, device_id={"cb": lax.rem(x + o, m)}, device_id_type=MESH)
    for copy in small:
        copy.wait()

    for l in range(2):
        floats = values[...].astype(f32)
        scaled[...] = (floats * gains[l]).astype(bf16)
        squares[l, z] = lax.dot_general(
            jnp.ones((8, width), f32), floats * floats, (((1,), (1,)), ((), ())),
            precision=lax.Precision.HIGHEST, preferred_element_type=f32)
        acc[...] = jnp.zeros_like(acc)
        if l == 0:
            pl.semaphore_wait(barrier, n + m - 2)
        for end in range(2):
            @pl.when(z != end * (n - 1))
            def _():
                sq_copy(l, end, z).start()

        def use_hidden(c, block):
            down_copy(l, c).wait()
            acc[...] += jnp.dot(block, w_down[l, c].astype(bf16), preferred_element_type=f32)

        def slot(s, carry):
            if l == 0:
                @pl.when(s < pairs)
                def _():
                    each_pair(s, lambda c: down_copy(0, c).start())

                @pl.when((s >= pairs) & (s < 2 * pairs))
                def _():
                    def act(c):
                        gate_copy(1, c).start()
                        up_copy(1, c).start()
                        down_copy(1, c).start()
                    each_pair(s - pairs, act)

            @pl.when(s < pairs)
            def _():
                def act(c):
                    gate_copy(l, c).wait()
                    up_copy(l, c).wait()
                    own[c] = jnp.dot(scaled[...], w_gu[l, c].astype(bf16), preferred_element_type=f32)
                each_pair(s, act)

            for d in range(2):
                p = place[d]
                k = s - LAG_SUM * p
                c = starts[d] + k
                turn = (k >= 0) & (k < counts[d])

                @pl.when(turn & (p == 0))
                def _():
                    sum_out[l, c] = own[c].astype(bf16)
                    sum_copy(l, c, d).start()

                @pl.when(turn & (p > 0) & (p < n - 1))
                def _():
                    sum_copy(l, c, d).wait_recv()
                    sum_out[l, c] = (own[c] + sum_in[l, c].astype(f32)).astype(bf16)
                    sum_copy(l, c, d).start()

                @pl.when(turn & (p == n - 1))
                def _():
                    @pl.when(k == 0)
                    def _():
                        for o in range(1, n):
                            sq_copy(l, 0, lax.rem(z + o, n)).wait_recv()
                        every = squares[l].reshape(8 * n, rows)
                        total = lax.dot_general(
                            every, jnp.full((8 * n, LANES), 0.125, f32), (((0,), (0,)), ((), ())),
                            precision=lax.Precision.HIGHEST, preferred_element_type=f32)
                        inverse[...] = lax.rsqrt(total / total_width + EPS)

                    sum_copy(l, c, d).wait_recv()
                    both = own[c] + sum_in[l, c].astype(f32)
                    inv = inverse[...]
                    g = both[:, :LANES] * gscales[l, :, columns(c)] * inv
                    u = both[:, LANES:] * uscales[l, :, columns(c)] * inv
                    block = (g / (1.0 + jnp.exp(-g)) * u).astype(bf16)
                    hid[l, c] = block
                    hid_copy(l, c, d).start()
                    use_hidden(c, block)

                k2 = s - LAG_SUM * (n - 1) - LAG_HID * (n - 1 - p)
                c2 = starts[d] + k2

                @pl.when((k2 >= 0) & (k2 < counts[d]) & (p < n - 1))
                def _():
                    hid_copy(l, c2, d).wait_recv()

                    @pl.when(p > 0)
                    def _():
                        hid_copy(l, c2, d).start()

                    use_hidden(c2, hid[l, c2])
            return carry

        lax.fori_loop(0, slots, slot, 0)

        down_in[l, x] = acc[...].astype(bf16)
        for o in range(1, m):
            part_copy(l, o, x).start()
        for o in range(1, m):
            part_copy(l, o, lax.rem(x + o, m)).wait_recv()
        total = down_in[l, 0].astype(f32)
        for o in range(1, m):
            total = total + down_in[l, o].astype(f32)
        result = (0.3 * values[...].astype(f32) + 0.5 * total * dscales[l]).astype(bf16)
        if l == 0:
            values[...] = result
        else:
            out[...] = result

    for l in range(2):
        for o in range(1, m):
            part_copy(l, o, x).wait_send()
        for end in range(2):
            @pl.when(z != end * (n - 1))
            def _():
                sq_copy(l, end, z).wait_send()
        for d in range(2):
            p = place[d]

            @pl.when(p < n - 1)
            def _():
                def body(k, carry):
                    sum_copy(l, starts[d] + k, d).wait_send()
                    return carry
                lax.fori_loop(0, counts[d], body, 0)

            @pl.when(p > 0)
            def _():
                def body(k, carry):
                    hid_copy(l, starts[d] + k, d).wait_send()
                    return carry
                lax.fori_loop(0, counts[d], body, 0)


def per_device(n, m, *args):
    tokens = args[0]
    rows, width = tokens.shape
    units = args[2].shape[1]
    blocks = units // LANES
    bf16, f32 = jnp.bfloat16, jnp.float32
    flat = [a.reshape(1, -1) if a.ndim == 1 else a for a in args]
    dma = pltpu.SemaphoreType.DMA
    return pl.pallas_call(
        functools.partial(kernel, (n, m, rows, width, units, n * width)),
        out_shape=jax.ShapeDtypeStruct((rows, width), bf16),
        in_specs=[pl.BlockSpec(memory_space=pl.ANY)] * len(flat),
        out_specs=pl.BlockSpec(memory_space=pltpu.VMEM),
        scratch_shapes=[
            pltpu.VMEM((rows, width), bf16),
            pltpu.VMEM((rows, width), bf16),
            pltpu.VMEM((2, 1, width), f32),
            pltpu.VMEM((2, 1, width), f32),
            pltpu.VMEM((2, 1, units), f32),
            pltpu.VMEM((2, 1, units), f32),
            pltpu.VMEM((2, blocks, width, 2 * LANES), f32),
            pltpu.VMEM((2, blocks, LANES, width), f32),
            pltpu.VMEM((blocks, rows, 2 * LANES), f32),
            pltpu.VMEM((2, blocks, rows, 2 * LANES), bf16),
            pltpu.VMEM((2, blocks, rows, 2 * LANES), bf16),
            pltpu.VMEM((2, blocks, rows, LANES), bf16),
            pltpu.VMEM((rows, width), f32),
            pltpu.VMEM((2, m, rows, width), bf16),
            pltpu.VMEM((2, n, 8, rows), f32),
            pltpu.VMEM((rows, LANES), f32),
            dma((9,)),
            dma((2, blocks)),
            dma((2, blocks)),
            dma((2, blocks)),
            dma((2, blocks)),
            dma((2, blocks)),
            dma((2, blocks)),
            dma((2, blocks)),
            dma((2, m)),
            dma((2, m)),
            dma((2, 2)),
            dma((2, n)),
        ],
        compiler_params=pltpu.CompilerParams(
            collective_id=0, has_side_effects=True, vmem_limit_bytes=60 * 1024 * 1024
        ),
    )(*flat)


def solution(mesh):
    in_specs = (
        P(("grp", "dp"), "ra"),
        P("ra"),
        P("ra", "cb"),
        P("ra", "cb"),
        P("cb", "ra"),
        P("cb"),
        P("cb"),
        P("ra"),
        P("ra"),
        P("ra", "cb"),
        P("ra", "cb"),
        P("cb", "ra"),
        P("cb"),
        P("cb"),
        P("ra"),
    )
    out_specs = P(("grp", "dp"), "ra")
    n, m = mesh.shape["ra"], mesh.shape["cb"]
    return jax.shard_map(
        functools.partial(per_device, n, m), mesh=mesh, in_specs=in_specs, out_specs=out_specs, check_vma=False
    )
```

time: 167 us -> 79.3 us (0.47)
  waiting for transfers between devices: 103 us -> 0 us
  Pallas kernels: 0 us -> 72.1 us
  blocking collectives: 25.6 us -> 0 us
  matrix products: 22.3 us -> 0 us
  between operations: 13.2 us -> 0.01 us
  local copies, waits for them, and re-layouts: 0.22 us -> 6.72 us
  other arithmetic: 2.6 us -> 0 us
    psum x4 -> x0, waiting for transfers between devices: 103 us -> none  [the longest x2 61.5 us: sublayer(): lax.psum(up_part.astype(jnp.bfloat16), 'ra').astype(jnp.float32)]
    pallas_call x0 -> x1, Pallas kernels: none -> 72.1 us  [per_device(): pl.pallas_call(functools.partial(kernel, (n, m, rows, width, units, n * w...]
    psum x2 -> x0, blocking collectives: 25.6 us -> none  [sublayer(): total = lax.psum(squares_row, 'ra')]
    dot_general x6 -> x0, matrix products: 22.3 us -> none  [the longest x2 8.7 us: sublayer(): jnp.dot(hidden, w_down.astype(jnp.bfloat16), preferred_element_type=jnp.f...]
    reshape x0 -> x4, local copies, waits for them, and re-layouts: none -> 5.24 us  [per_device(): flat = [a.reshape(1, -1) if a.ndim == 1 else a for a in args]]
  transfers between devices with their start and end apart: 4 -> 0, of which waited for: 4 -> 0; matrix products, arithmetic and copies ran while one was open for 0% -> 0% of each run, Pallas kernels for 0% -> 0%
where the time goes in v1:
time: 79.3 us; the launch traced here: 78.8 us
  Pallas kernels  72.1 us (91%)
  local copies, waits for them, and re-layouts  6.72 us (8%)
    pallas_call x1, Pallas kernels, per_device(): pl.pallas_call(functools.partial(kernel, (n, m, rows, width, units, n * w...  72.1 us
    reshape x4, local copies, waits for them, and re-layouts, per_device(): flat = [a.reshape(1, -1) if a.ndim == 1 else a for a in args]  5.24 us

profile of v1, /device:TPU:0, one launch (start us, length us, event | category | flops | bytes accessed | tf_op | source)
XLA Modules:
  0.0 78.8 jit_solution(1464069026572199743)
XLA Ops:
  0.0 1.3 %reshape.25.refs_5_ = f32[1,2816]{1,0:T(1,128)} reshape(f32[2816]{0:T(1024)} %param.20) | data formatting | bytes 22528 | tf_op jit(solution)/shard_map/reshape | solution.py:247
  1.3 1.3 %reshape.26.refs_6_ = f32[1,2816]{1,0:T(1,128)} reshape(f32[2816]{0:T(1024)} %param.21) | data formatting | bytes 22528 | tf_op jit(solution)/shard_map/reshape | solution.py:247
  2.6 1.3 %reshape.29.refs_12_ = f32[1,2816]{1,0:T(1,128)} reshape(f32[2816]{0:T(1024)} %param.27) | data formatting | bytes 22528 | tf_op jit(solution)/shard_map/reshape | solution.py:247
  3.9 1.3 %reshape.30.refs_13_ = f32[1,2816]{1,0:T(1,128)} reshape(f32[2816]{0:T(1024)} %param.28) | data formatting | bytes 22528 | tf_op jit(solution)/shard_map/reshape | solution.py:247
  5.2 72.1 %shard_map.145 = bf16[64,512]{1,0:T(8,128)(2,1)} custom-call(bf16[64,512]{1,0:T(8,128)(2,1)} %refs_0_.1, f32[1,512]{1,0:T(1,128)} %bitcast.4, f32[512,2816]{1,0:T(8,128)} %refs_2_.1, f32[512,2816]{1,0:T(8,128)} %refs_3_.1, f32[2816,512]{1,0:T(8,128)} %refs_4_.1, f32[1,2816]{1,0:T(1,128)} %reshape.25.refs_5_, f32[1,2816]{1,0:T(1,128)} %reshape.26.refs_6_, ...), custom_call_target="tpu_custom_call" | custom-call | tf_op jit(solution)/shard_map/pallas_call | solution.py:249
  77.4 1.5 %copy.17 = bf16[64,512]{1,0:T(8,128)(2,1)} copy(bf16[64,512]{1,0:T(8,128)(2,1)} %shard_map.145) | data formatting | bytes 131072

commit v2 on v1

v2 whole, which is shorter than its diff:
```python
import functools

import jax
import jax.numpy as jnp
from jax import lax
from jax.experimental import pallas as pl
from jax.experimental.pallas import tpu as pltpu
from jax.sharding import PartitionSpec as P

EPS = 1e-06
MESH = pl.DeviceIdType.MESH
LANES = 128
LAG_SUM = 5
LAG_HID = 8


def kernel(dims, *refs):
    n, m, rows, width, units, total_width = dims
    (tokens, gain0, gate0, up0, down0, gs0, us0, ds0, gain1, gate1, up1, down1, gs1, us1, ds1) = refs[:15]
    out = refs[15]
    (values, scaled, gains, dscales, gscales, uscales, w_gu, w_down, own, sum_out, sum_in, cross_in, hid, acc,
     down_in, squares, inverse, small_sem, gate_sem, up_sem, down_sem, sum_ss, sum_rs, cross_rs, hid_ss, hid_rs,
     part_ss, part_rs, sq_ss, sq_rs) = refs[16:]
    gate, up, down = (gate0, gate1), (up0, up1), (down0, down1)
    bf16, f32 = jnp.bfloat16, jnp.float32

    z, x = lax.axis_index("ra"), lax.axis_index("cb")
    blocks = units // LANES
    half = n // 2
    owners = (half - 1, half)
    counts = (blocks - blocks // 2, blocks // 2)
    starts = (0, counts[0])
    left = z < half
    step = jnp.where(left, 1, -1)
    p = jnp.where(left, z, n - 1 - z)
    middle = (z == half - 1) | (z == half)
    first = jnp.where(left, counts[0], 0)
    n_far = jnp.where(left, counts[1], counts[0])
    depth = (half - 1, n - half - 1)
    slots = max(blocks + blocks // 2, blocks + LAG_SUM * max(depth) + LAG_HID)

    def copy_small():
        found = []
        for i, (src, dst) in enumerate((
            (tokens, values), (gain0, gains.at[0]), (gs0, gscales.at[0]), (us0, uscales.at[0]), (ds0, dscales.at[0]),
            (gain1, gains.at[1]), (gs1, gscales.at[1]), (us1, uscales.at[1]), (ds1, dscales.at[1]),
        )):
            found.append(pltpu.make_async_copy(src, dst, small_sem.at[i]))
        return found

    def columns(c):
        return pl.ds(pl.multiple_of(c * LANES, LANES), LANES)

    def gate_copy(l, c):
        return pltpu.make_async_copy(gate[l].at[:, columns(c)], w_gu.at[l, c, :, pl.ds(0, LANES)], gate_sem.at[l, c])

    def up_copy(l, c):
        return pltpu.make_async_copy(up[l].at[:, columns(c)], w_gu.at[l, c, :, pl.ds(LANES, LANES)], up_sem.at[l, c])

    def down_copy(l, c):
        return pltpu.make_async_copy(down[l].at[columns(c), :], w_down.at[l, c], down_sem.at[l, c])

    def sum_copy(l, c):
        return pltpu.make_async_remote_copy(
            src_ref=sum_out.at[l, c], dst_ref=sum_in.at[l, c], send_sem=sum_ss.at[l, c], recv_sem=sum_rs.at[l, c],
            device_id={"ra": z + step}, device_id_type=MESH)

    def cross_copy(l, c):
        return pltpu.make_async_remote_copy(
            src_ref=sum_out.at[l, c], dst_ref=cross_in.at[l, c], send_sem=sum_ss.at[l, c],
            recv_sem=cross_rs.at[l, c], device_id={"ra": z + step}, device_id_type=MESH)

    def hid_copy(l, c, o):
        return pltpu.make_async_remote_copy(
            src_ref=hid.at[l, c], dst_ref=hid.at[l, c], send_sem=hid_ss.at[l, o, c], recv_sem=hid_rs.at[l, c],
            device_id={"ra": lax.rem(z + o, n)}, device_id_type=MESH)

    def part_copy(l, o, sender):
        return pltpu.make_async_remote_copy(
            src_ref=down_in.at[l, sender], dst_ref=down_in.at[l, sender], send_sem=part_ss.at[l, o],
            recv_sem=part_rs.at[l, sender], device_id={"cb": lax.rem(x + o, m)}, device_id_type=MESH)

    def sq_copy(l, end, sender):
        return pltpu.make_async_remote_copy(
            src_ref=squares.at[l, sender], dst_ref=squares.at[l, sender], send_sem=sq_ss.at[l, end],
            recv_sem=sq_rs.at[l, sender], device_id={"ra": owners[end]}, device_id_type=MESH)

    def stream(j):
        return lax.rem(first + j, blocks)

    small = copy_small()
    for copy in small:
        copy.start()

    def start_first(i, carry):
        c = stream(i)
        gate_copy(0, c).start()
        up_copy(0, c).start()
        return carry

    lax.fori_loop(0, blocks, start_first, 0)

    barrier = pltpu.get_barrier_semaphore()
    for o in range(1, n):
        pl.semaphore_signal(barrier, inc=1, device_id={"ra": lax.rem(z + o, n)}, device_id_type=MESH)
    for o in range(1, m):
        pl.semaphore_signal(barrier, inc=1, device_id={"cb": lax.rem(x + o, m)}, device_id_type=MESH)
    for copy in small:
        copy.wait()

    for l in range(2):
        floats = values[...].astype(f32)
        scaled[...] = (floats * gains[l]).astype(bf16)
        squares[l, z] = lax.dot_general(
            jnp.ones((8, width), f32), floats * floats, (((1,), (1,)), ((), ())),
            precision=lax.Precision.HIGHEST, preferred_element_type=f32)
        acc[...] = jnp.zeros_like(acc)
        if l == 0:
            pl.semaphore_wait(barrier, n + m - 2)
        for end in range(2):
            @pl.when(z != owners[end])
            def _():
                sq_copy(l, end, z).start()

        def use_hidden(c, block):
            down_copy(l, c).wait()
            acc[...] += jnp.dot(block, w_down[l, c].astype(bf16), preferred_element_type=f32)

        def slot(s, carry):
            if l == 0:
                @pl.when(s < blocks)
                def _():
                    down_copy(0, stream(s)).start()

                later = s - blocks // 2

                @pl.when((later >= 0) & (later < blocks))
                def _():
                    c = stream(later)
                    gate_copy(1, c).start()
                    up_copy(1, c).start()
                    down_copy(1, c).start()

            @pl.when(s < blocks)
            def _():
                c = stream(s)
                gate_copy(l, c).wait()
                up_copy(l, c).wait()
                own[c] = jnp.dot(scaled[...], w_gu[l, c].astype(bf16), preferred_element_type=f32)

            k = s - LAG_SUM * p
            c = stream(jnp.clip(k, 0, blocks - 1))
            turn = (k >= 0) & (k < blocks)
            mine = middle & (k >= n_far)

            @pl.when(turn & jnp.logical_not(mine))
            def _():
                @pl.when(p == 0)
                def _():
                    sum_out[l, c] = own[c].astype(bf16)

                @pl.when(p > 0)
                def _():
                    sum_copy(l, c).wait_recv()
                    sum_out[l, c] = (own[c] + sum_in[l, c].astype(f32)).astype(bf16)

                @pl.when(middle)
                def _():
                    cross_copy(l, c).start()

                @pl.when(jnp.logical_not(middle))
                def _():
                    sum_copy(l, c).start()

            @pl.when(turn & mine)
            def _():
                @pl.when(k == n_far)
                def _():
                    for o in range(1, n):
                        sq_copy(l, 0, lax.rem(z + o, n)).wait_recv()
                    every = squares[l].reshape(8 * n, rows)
                    total = lax.dot_general(
                        every, jnp.full((8 * n, LANES), 0.125, f32), (((0,), (0,)), ((), ())),
                        precision=lax.Precision.HIGHEST, preferred_element_type=f32)
                    inverse[...] = lax.rsqrt(total / total_width + EPS)

                @pl.when(p > 0)
                def _():
                    sum_copy(l, c).wait_recv()
                    own[c] += sum_in[l, c].astype(f32)

                cross_copy(l, c).wait_recv()
                both = own[c] + cross_in[l, c].astype(f32)
                inv = inverse[...]
                g = both[:, :LANES] * gscales[l, pl.ds(c, 1), :] * inv
                u = both[:, LANES:] * uscales[l, pl.ds(c, 1), :] * inv
                block = (g / (1.0 + jnp.exp(-g)) * u).astype(bf16)
                hid[l, c] = block
                for o in range(1, n):
                    hid_copy(l, c, o).start()
                use_hidden(c, block)

            for d in range(2):
                k2 = s - counts[1 - d] - LAG_SUM * depth[d] - LAG_HID

                @pl.when((k2 >= 0) & (k2 < counts[d]) & (z != owners[d]))
                def _():
                    c2 = starts[d] + k2
                    hid_copy(l, c2, 1).wait_recv()
                    use_hidden(c2, hid[l, c2])
            return carry

        lax.fori_loop(0, slots, slot, 0)

        down_in[l, x] = acc[...].astype(bf16)
        for o in range(1, m):
            part_copy(l, o, x).start()
        for o in range(1, m):
            part_copy(l, o, lax.rem(x + o, m)).wait_recv()
        total = down_in[l, 0].astype(f32)
        for o in range(1, m):
            total = total + down_in[l, o].astype(f32)
        result = (0.3 * values[...].astype(f32) + 0.5 * total * dscales[l]).astype(bf16)
        if l == 0:
            values[...] = result
        else:
            out[...] = result

    for l in range(2):
        for o in range(1, m):
            part_copy(l, o, x).wait_send()
        for end in range(2):
            @pl.when(z != owners[end])
            def _():
                sq_copy(l, end, z).wait_send()
        def sent_sum(k, carry):
            sum_copy(l, stream(k)).wait_send()
            return carry

        lax.fori_loop(0, jnp.where(middle, n_far, blocks), sent_sum, 0)

        @pl.when(middle)
        def _():
            def sent_hid(k, carry):
                for o in range(1, n):
                    hid_copy(l, stream(n_far + k), o).wait_send()
                return carry
            lax.fori_loop(0, blocks - n_far, sent_hid, 0)


def per_device(n, m, *args):
    tokens = args[0]
    rows, width = tokens.shape
    units = args[2].shape[1]
    blocks = units // LANES
    bf16, f32 = jnp.bfloat16, jnp.float32
    flat = [a if a.ndim > 1 else a.reshape(1, width) if i in (1, 7, 8, 14) else a.reshape(blocks, LANES) for i, a in enumerate(args)]
    dma = pltpu.SemaphoreType.DMA
    return pl.pallas_call(
        functools.partial(kernel, (n, m, rows, width, units, n * width)),
        out_shape=jax.ShapeDtypeStruct((rows, width), bf16),
        in_specs=[pl.BlockSpec(memory_space=pl.ANY)] * len(flat),
        out_specs=pl.BlockSpec(memory_space=pltpu.VMEM),
        scratch_shapes=[
            pltpu.VMEM((rows, width), bf16),
            pltpu.VMEM((rows, width), bf16),
            pltpu.VMEM((2, 1, width), f32),
            pltpu.VMEM((2, 1, width), f32),
            pltpu.VMEM((2, blocks, LANES), f32),
            pltpu.VMEM((2, blocks, LANES), f32),
            pltpu.VMEM((2, blocks, width, 2 * LANES), f32),
            pltpu.VMEM((2, blocks, LANES, width), f32),
            pltpu.VMEM((blocks, rows, 2 * LANES), f32),
            pltpu.VMEM((2, blocks, rows, 2 * LANES), bf16),
            pltpu.VMEM((2, blocks, rows, 2 * LANES), bf16),
            pltpu.VMEM((2, blocks, rows, 2 * LANES), bf16),
            pltpu.VMEM((2, blocks, rows, LANES), bf16),
            pltpu.VMEM((rows, width), f32),
            pltpu.VMEM((2, m, rows, width), bf16),
            pltpu.VMEM((2, n, 8, rows), f32),
            pltpu.VMEM((rows, LANES), f32),
            dma((9,)),
            dma((2, blocks)),
            dma((2, blocks)),
            dma((2, blocks)),
            dma((2, blocks)),
            dma((2, blocks)),
            dma((2, blocks)),
            dma((2, n, blocks)),
            dma((2, blocks)),
            dma((2, m)),
            dma((2, m)),
            dma((2, 2)),
            dma((2, n)),
        ],
        compiler_params=pltpu.CompilerParams(
            collective_id=0, has_side_effects=True, vmem_limit_bytes=60 * 1024 * 1024
        ),
    )(*flat)


def solution(mesh):
    in_specs = (
        P(("grp", "dp"), "ra"),
        P("ra"),
        P("ra", "cb"),
        P("ra", "cb"),
        P("cb", "ra"),
        P("cb"),
        P("cb"),
        P("ra"),
        P("ra"),
        P("ra", "cb"),
        P("ra", "cb"),
        P("cb", "ra"),
        P("cb"),
        P("cb"),
        P("ra"),
    )
    out_specs = P(("grp", "dp"), "ra")
    n, m = mesh.shape["ra"], mesh.shape["cb"]
    return jax.shard_map(
        functools.partial(per_device, n, m), mesh=mesh, in_specs=in_specs, out_specs=out_specs, check_vma=False
    )
```

time: 79.3 us -> 59.6 us (0.75)
  Pallas kernels: 72.1 us -> 58 us
  local copies, waits for them, and re-layouts: 6.72 us -> 1.47 us
    pallas_call x1, Pallas kernels: 72.1 us -> 58 us  [per_device(): pl.pallas_call(functools.partial(kernel, (n, m, rows, width, units, n * w...]
    reshape x4 -> x0, local copies, waits for them, and re-layouts: 5.24 us -> none  [per_device(): flat = [a.reshape(1, -1) if a.ndim == 1 else a for a in args]]
where the time goes in v2:
time: 59.6 us; the launch traced here: 59.5 us
  Pallas kernels  58 us (97%)
  local copies, waits for them, and re-layouts  1.47 us (2%)
    pallas_call x1, Pallas kernels, per_device(): pl.pallas_call(functools.partial(kernel, (n, m, rows, width, units, n * w...  58 us
    unnamed x1, local copies, waits for them, and re-layouts  1.47 us

profile of v2, /device:TPU:0, one launch (start us, length us, event | category | flops | bytes accessed | tf_op | source)
XLA Modules:
  0.0 59.5 jit_solution(4634393250569619335)
XLA Ops:
  0.0 58.0 %shard_map.145 = bf16[64,512]{1,0:T(8,128)(2,1)} custom-call(bf16[64,512]{1,0:T(8,128)(2,1)} %refs_0_.1, f32[1,512]{1,0:T(1,128)} %bitcast.12, f32[512,2816]{1,0:T(8,128)} %refs_2_.1, f32[512,2816]{1,0:T(8,128)} %refs_3_.1, f32[2816,512]{1,0:T(8,128)} %refs_4_.1, f32[22,128]{1,0:T(8,128)} %bitcast.8, f32[22,128]{1,0:T(8,128)} %bitcast.9, f32[1,512]{1,0:T(1,128)} %bitcast.13, ...), custom_call_target="tpu_custom_call" | custom-call | tf_op jit(solution)/shard_map/pallas_call | solution.py:259
  58.0 1.5 %copy.17 = bf16[64,512]{1,0:T(8,128)(2,1)} copy(bf16[64,512]{1,0:T(8,128)(2,1)} %shard_map.145) | data formatting | bytes 131072
